TPU v7x, 32 devices: a whole 2x2x4 slice. The times are simulated.
32 devices in a mesh: sp: 8 (over z, x), tp: 4 (over y, core).
Axes of the slice: x: 2, y: 2, z: 4, core: 2. Of those that a mesh axis runs over, the one named last changes fastest.
Arguments:
- layer_grad: bfloat16 [2048, 2048], P('sp', 'tp'), may hold values from -6 to 6
- routes: int32 [2048, 2], P('sp'), may hold values from 0 to 7, all different within a row; in each aligned block of 256 rows (0 to 255, 256 to 511, ...) at most 96 rows name the same one
- route_weights: float32 [2048, 2], P('sp'), may hold values from 0.1 to 0.9
- expert_in: bfloat16 [8, 768, 2048], P('sp', None, 'tp'), may hold values from -50 to 50
- w_gate: bfloat16 [8, 2048, 2048], P('sp', None, 'tp'), may hold values from -0.125 to 0.125
- w_up: bfloat16 [8, 2048, 2048], P('sp', None, 'tp'), may hold values from -0.125 to 0.125
- w_down: bfloat16 [8, 2048, 2048], P('sp', 'tp'), may hold values from -0.125 to 0.125
- conv_in: bfloat16 [2048, 512], P('sp', 'tp'), may hold values from -6 to 6
- c_gate: bfloat16 [2048, 512], P('sp', 'tp'), may hold values from -6 to 6
- b_gate: bfloat16 [2048, 512], P('sp', 'tp'), may hold values from -1.5 to 1.5
- conv_out: bfloat16 [2048, 512], P('sp', 'tp'), may hold values from -1.5 to 1.5
- taps: bfloat16 [3, 512], P(None, 'tp'), may hold values from -3.5 to 3.5
- w_out: bfloat16 [512, 2048], P('tp'), may hold values from -0.25 to 0.25
Outputs:
- grad_w_gate: bfloat16 [8, 2048, 2048], P('sp', None, 'tp')
- grad_w_up: bfloat16 [8, 2048, 2048], P('sp', None, 'tp')
- grad_w_down: bfloat16 [8, 2048, 2048], P('sp', 'tp')
- grad_routed: bfloat16 [2048, 2048], P('sp', 'tp')
- grad_out_proj: float32 [512, 2048], P('tp', 'sp')
- grad_conv_in: bfloat16 [2048, 512], P('sp', 'tp')
- grad_c_gate: bfloat16 [2048, 512], P('sp', 'tp')
- grad_b_gate: bfloat16 [2048, 512], P('sp', 'tp')
Inputs may be any that keep to these rules, and one draw needn't show every extreme that they name: `routes`: each token names 2 different experts. Among the tokens of one block of 256, no expert is named more than 96 times, a bound that some block reaches.
All inputs are finite; a program needn't handle non-finite values.
Results may differ from a plain program's by a relative error of at most 0.019.
Values may be sent and summed in bfloat16 or wider, within the bound.
A program may use at most 64 MiB of HBM per device.

v0:
```python
import functools

import jax
import jax.numpy as jnp
from jax import lax
from jax.experimental import pallas as pl
from jax.experimental.pallas import tpu as pltpu
from jax.sharding import PartitionSpec as P

clamp_limit = 7.0
swish_alpha = 1.702


def passed_along(value, axis, steps):
    count = lax.axis_size(axis)
    leading, last = (max(0, -steps), min(count, count - steps))
    return lax.ppermute(value, axis, [(source, source + steps) for source in range(leading, last)])


def per_device(
    layer_grad,
    routes,
    route_weights,
    expert_in,
    w_gate,
    w_up,
    w_down,
    conv_in,
    c_gate,
    b_gate,
    conv_out,
    taps,
    w_out,
):
    sp_devices = lax.axis_size("sp")
    tok_rows = layer_grad.shape[0]
    top_count = routes.shape[1]
    capacity = expert_in.shape[1] // sp_devices
    full_grad = lax.all_gather(layer_grad, "tp", axis=1, tiled=True)
    flat_routes = routes.reshape(-1)
    onehot = (flat_routes[:, None] == jnp.arange(sp_devices, dtype=jnp.int32)[None, :]).astype(
        jnp.int32
    )
    slot_rank = jnp.sum((jnp.cumsum(onehot, axis=0) - 1) * onehot, axis=1)
    slot_index = flat_routes * capacity + slot_rank
    weights = route_weights[:, :, None]
    scaled = (weights * layer_grad[:, None, :].astype(jnp.float32)).astype(jnp.bfloat16)
    scaled = scaled.reshape(tok_rows * top_count, -1)
    buffer = (
        jnp.zeros((sp_devices * capacity, scaled.shape[1]), jnp.bfloat16).at[slot_index].set(scaled)
    )
    arrived = lax.all_to_all(
        buffer.reshape(sp_devices, capacity, -1), "sp", split_axis=0, concat_axis=0, tiled=True
    )
    expert_grad, saved_rows = (
        lax.all_gather(arrived.reshape(sp_devices * capacity, -1), "tp", axis=1, tiled=True),
        lax.all_gather(expert_in[0], "tp", axis=1, tiled=True),
    )
    gate_weight = w_gate[0]
    up_weight = w_up[0]
    down_weight = w_down[0]
    gate_pre = jnp.dot(saved_rows, gate_weight, preferred_element_type=jnp.float32)
    up_pre = jnp.dot(saved_rows, up_weight, preferred_element_type=jnp.float32)
    gate_cut = jnp.minimum(gate_pre, clamp_limit)
    up_cut = jnp.clip(up_pre, -clamp_limit, clamp_limit)
    sigmoid_gate = jax.nn.sigmoid(swish_alpha * gate_cut)
    hidden = ((up_cut + 1.0) * gate_cut * sigmoid_gate).astype(jnp.bfloat16)
    act_grad = jnp.einsum("rd,fd->rf", expert_grad, down_weight, preferred_element_type=jnp.float32)
    grad_down = jnp.einsum(
        "rf,rd->fd", hidden, expert_grad, preferred_element_type=jnp.float32
    ).astype(jnp.bfloat16)
    slope = sigmoid_gate + swish_alpha * gate_cut * sigmoid_gate * (1.0 - sigmoid_gate)
    gate_grad = jnp.where(gate_pre < clamp_limit, act_grad * (up_cut + 1.0) * slope, 0.0).astype(
        jnp.bfloat16
    )
    up_grad = jnp.where(
        jnp.abs(up_pre) < clamp_limit, act_grad * gate_cut * sigmoid_gate, 0.0
    ).astype(jnp.bfloat16)
    grad_gate = jnp.einsum(
        "rd,rf->df", saved_rows, gate_grad, preferred_element_type=jnp.float32
    ).astype(jnp.bfloat16)
    grad_up = jnp.einsum(
        "rd,rf->df", saved_rows, up_grad, preferred_element_type=jnp.float32
    ).astype(jnp.bfloat16)
    partial_value = jnp.einsum(
        "rf,df->rd", gate_grad, gate_weight, preferred_element_type=jnp.float32
    )
    partial_value = partial_value + jnp.einsum(
        "rf,df->rd", up_grad, up_weight, preferred_element_type=jnp.float32
    )
    rounded_terms = partial_value.astype(jnp.bfloat16)
    reduced = (
        lax.psum_scatter(rounded_terms, "tp", scatter_dimension=1, tiled=True)
        .astype(jnp.float32)
        .astype(jnp.bfloat16)
    )
    returned = lax.all_to_all(
        reduced.reshape(sp_devices, capacity, -1), "sp", split_axis=0, concat_axis=0, tiled=True
    )
    returned = returned.reshape(sp_devices * capacity, -1)
    picked = returned[slot_index]
    picked = picked.reshape(tok_rows, top_count, -1)
    grad_routed = jnp.sum(picked.astype(jnp.float32), axis=1).astype(jnp.bfloat16)
    mixer_grad = jnp.einsum("td,cd->tc", full_grad, w_out, preferred_element_type=jnp.float32)
    mixed = (b_gate.astype(jnp.float32) * conv_out.astype(jnp.float32)).astype(jnp.bfloat16)
    projected = lax.psum_scatter(
        jnp.einsum("td,tc->dc", full_grad, mixed, preferred_element_type=jnp.float32),
        "sp",
        scatter_dimension=0,
        tiled=True,
    )
    grad_out_proj = projected.T
    out_grad = mixer_grad * b_gate.astype(jnp.float32)
    tap_reach = taps.shape[0] - 1
    following = passed_along(out_grad[:tap_reach], "sp", -1)
    extended = jnp.concatenate([out_grad, following], axis=0)
    tap_values = taps.astype(jnp.float32)
    conv_grad = jnp.zeros_like(out_grad)
    for tap_index in range(tap_reach + 1):
        offset = tap_reach - tap_index
        conv_grad = conv_grad + tap_values[tap_index] * extended[offset : offset + tok_rows]
    grad_conv_in = (conv_grad * c_gate.astype(jnp.float32)).astype(jnp.bfloat16)
    grad_c_gate = (conv_grad * conv_in.astype(jnp.float32)).astype(jnp.bfloat16)
    grad_b_gate = (mixer_grad * conv_out.astype(jnp.float32)).astype(jnp.bfloat16)
    return (
        grad_gate[None],
        grad_up[None],
        grad_down[None],
        grad_routed,
        grad_out_proj,
        grad_conv_in,
        grad_c_gate,
        grad_b_gate,
    )


MESH = pl.DeviceIdType.MESH
bf16 = jnp.bfloat16
f32 = jnp.float32


def dot_nn(a, b):
    return jnp.dot(a, b, preferred_element_type=f32)


def dot_nt(a, b):
    return lax.dot_general(a, b, (((1,), (1,)), ((), ())), preferred_element_type=f32)


def dot_tn(a, b):
    return lax.dot_general(a, b, (((0,), (0,)), ((), ())), preferred_element_type=f32)


def fused_kernel(
    n_sp,
    lg_hbm,
    rt_ref,
    wt_ref,
    ein_hbm,
    wg_hbm,
    wu_hbm,
    wd_hbm,
    ci_ref,
    cg_ref,
    bg_ref,
    co_ref,
    taps_ref,
    wo_hbm,
    gg_v,
    gu_v,
    gd_v,
    gr_ref,
    gop_ref,
    gci_ref,
    gcg_ref,
    gbg_ref,
    wg,
    wu,
    wd,
    wo,
    fg,
    saved,
    saved_t,
    eg,
    disp,
    sel,
    proj,
    precv,
    ext,
    halo,
    hidden_t,
    fac_g,
    fac_u,
    ggrad,
    ugrad,
    terms,
    px,
    ysend,
    yrecv,
    red,
    ret,
    load_s,
    lg_s,
    lg_r,
    ein_s,
    ein_r,
    disp_s,
    disp_r,
    egs_s,
    egs_r,
    proj_s,
    proj_r,
    halo_s,
    halo_r,
    d2d_s,
    d2d_r,
    y_s,
    y_r,
    ret_s,
    ret_r,
):
    sp = lax.axis_index("sp")
    tp = lax.axis_index("tp")
    core, chip = lax.rem(tp, 2), lax.div(tp, 2)
    partner = chip * 2 + (1 - core)
    across = (1 - chip) * 2 + core
    plane, side = lax.div(sp, 2), lax.rem(sp, 2)
    planes = n_sp // 2
    rows, dcols = ein_hbm.shape
    cap = rows // n_sp
    pair = 2 * cap
    width = fg.shape[1]
    tokens = fg.shape[0]
    units = wg.shape[1]
    top = rt_ref.shape[0]

    def cols(j):
        return pl.ds(pl.multiple_of(j * dcols, dcols), dcols)

    def block(b):
        return pl.ds(pl.multiple_of(b * cap, cap), cap)

    def pair_rows(q):
        return pl.ds(pl.multiple_of(q * pair, pair), pair)

    mine = cols(tp)

    def load(src, dst, n):
        copy = pltpu.make_async_copy(src, dst, load_s.at[n])
        copy.start()
        return copy

    def remote(src, dst, send, recv, to_sp, to_tp):
        return pltpu.make_async_remote_copy(
            src_ref=src,
            dst_ref=dst,
            send_sem=send,
            recv_sem=recv,
            device_id=(to_sp, to_tp),
            device_id_type=MESH,
        )

    lg_load = load(lg_hbm, fg.at[:, mine], 0)
    ein_load = load(ein_hbm, saved.at[:, mine], 1)
    wo_load = load(wo_hbm, wo, 2)
    wg_load = load(wg_hbm, wg, 3)
    wu_load = load(wu_hbm, wu, 4)
    wd_load = load(wd_hbm, wd, 5)

    barrier = pltpu.get_barrier_semaphore()
    pl.semaphore_signal(barrier, inc=1, device_id=(sp, partner), device_id_type=MESH)
    pl.semaphore_signal(barrier, inc=1, device_id=(sp, across), device_id_type=MESH)
    for i in range(1, n_sp):
        pl.semaphore_signal(
            barrier, inc=1, device_id=(lax.rem(sp + i, n_sp), tp), device_id_type=MESH
        )
    pl.semaphore_wait(barrier, n_sp + 1)

    pending = []

    def send(copy):
        copy.start()
        pending.append(copy)
        return copy

    def gather(src, buf, sl, s_sem, r_sem, base):
        send(remote(src, buf.at[sl, mine], s_sem.at[base], r_sem.at[base], sp, across))
        send(remote(src, buf.at[sl, mine], s_sem.at[base + 1], r_sem.at[base + 1], sp, partner))

    def relay(buf, sl, s_sem, r_sem, base):
        region = buf.at[sl, cols(across)]
        remote(region, region, s_sem.at[base], r_sem.at[base], sp, across).wait_recv()
        send(remote(region, region, s_sem.at[base + 2], r_sem.at[base + 2], sp, partner))

    def arrive(buf, sl, s_sem, r_sem, base):
        region = buf.at[sl, cols(partner)]
        remote(region, region, s_sem.at[base + 1], r_sem.at[base + 1], sp, partner).wait_recv()
        last = buf.at[sl, cols((1 - chip) * 2 + (1 - core))]
        remote(last, last, s_sem.at[base + 2], r_sem.at[base + 2], sp, partner).wait_recv()

    gather(lg_hbm, fg, pl.ds(0, tokens), lg_s, lg_r, 0)
    gather(ein_hbm, saved, pl.ds(0, rows), ein_s, ein_r, 0)

    expert_ids = lax.broadcasted_iota(jnp.int32, (n_sp, tokens), 0)
    named = jnp.zeros((n_sp, tokens), f32)
    weight = jnp.zeros((n_sp, tokens), f32)
    for k in range(top):
        hit = rt_ref[k : k + 1, :] == expert_ids
        named = jnp.where(hit, 1.0, named)
        weight = jnp.where(hit, wt_ref[k : k + 1, :], weight)
    earlier = (
        lax.broadcasted_iota(jnp.int32, (tokens, tokens), 0)
        < lax.broadcasted_iota(jnp.int32, (tokens, tokens), 1)
    )
    rank = dot_nn(named.astype(bf16), jnp.where(earlier, 1.0, 0.0).astype(bf16))
    rank = jnp.where(named > 0.0, rank, -1.0)
    slots = lax.broadcasted_iota(jnp.int32, (cap, tokens), 0).astype(f32)
    lg_load.wait()
    own_grad = fg[:, mine]
    for e in range(n_sp):
        chosen = slots == rank[e : e + 1, :]
        picks = jnp.where(chosen, 1.0, 0.0)
        row_weight = jnp.sum(jnp.where(chosen, weight[e : e + 1, :], 0.0), axis=1, keepdims=True)
        sel[e * cap : (e + 1) * cap, :] = picks.astype(bf16)
        disp[e * cap : (e + 1) * cap, :] = (
            dot_nn(picks.astype(bf16), own_grad) * row_weight
        ).astype(bf16)

    def dispatch(dest):
        send(
            remote(
                disp.at[block(dest), :],
                eg.at[block(sp), mine],
                disp_s.at[dest],
                disp_r.at[sp],
                dest,
                tp,
            )
        )

    dispatch(plane * 2 + (1 - side))
    for i in range(1, planes):
        there = lax.rem(plane - i + planes, planes)
        for x in range(2):
            dispatch(there * 2 + x)
    eg[block(sp), mine] = disp[block(sp), :]

    whole_tokens = pl.ds(0, tokens)
    relay(fg, whole_tokens, lg_s, lg_r, 0)
    wo_load.wait()
    arrive(fg, whole_tokens, lg_s, lg_r, 0)
    b_gate = bg_ref[...].astype(f32)
    conv_out = co_ref[...].astype(f32)
    mixer_grad = dot_nt(fg[...], wo[...])
    out_grad = mixer_grad * b_gate
    ext[0:tokens, :] = out_grad
    gbg_ref[...] = (mixer_grad * conv_out).astype(bf16)
    before = lax.rem(sp + n_sp - 1, n_sp)
    halo_copy = send(remote(ext.at[0:8, :], halo, halo_s, halo_r, before, tp))
    mixed = (b_gate * conv_out).astype(bf16)
    share = width // n_sp
    for d in range(n_sp):
        proj[d] = dot_tn(mixed, fg[:, d * share : (d + 1) * share])
    for i in range(1, n_sp):
        dest = lax.rem(sp - i + n_sp, n_sp)
        send(remote(proj.at[dest], precv.at[sp], proj_s.at[dest], proj_r.at[sp], dest, tp))

    def arrived(source):
        region = eg.at[block(source), mine]
        remote(region, region, disp_s.at[source], disp_r.at[source], source, tp).wait_recv()

    order = [lax.rem(plane + i, planes) for i in range(planes)]
    for i in range(planes):
        if i == 0:
            arrived(plane * 2 + (1 - side))
        else:
            arrived(order[i] * 2)
            arrived(order[i] * 2 + 1)
        gather(eg.at[pair_rows(order[i]), mine], eg, pair_rows(order[i]), egs_s, egs_r, 3 * i)

    ein_load.wait()
    whole_rows = pl.ds(0, rows)
    relay(saved, whole_rows, ein_s, ein_r, 0)
    wg_load.wait()
    wu_load.wait()
    arrive(saved, whole_rows, ein_s, ein_r, 0)

    def forward(r, carry):
        sl = pl.ds(pl.multiple_of(r * pair, pair), pair)
        x = saved[sl, :]
        gate_pre = dot_nn(x, wg[...])
        up_pre = dot_nn(x, wu[...])
        gate_cut = jnp.minimum(gate_pre, clamp_limit)
        up_cut = jnp.clip(up_pre, -clamp_limit, clamp_limit)
        sig = jax.nn.sigmoid(swish_alpha * gate_cut)
        base = gate_cut * sig
        slope = sig + swish_alpha * base * (1.0 - sig)
        disp2 = ((up_cut + 1.0) * base).astype(bf16)
        ggrad[sl, :] = disp2
        fac_g[sl, :] = jnp.where(gate_pre < clamp_limit, (up_cut + 1.0) * slope, 0.0)
        fac_u[sl, :] = jnp.where(jnp.abs(up_pre) < clamp_limit, base, 0.0)
        return carry

    lax.fori_loop(0, planes, forward, 0)
    hidden_t[...] = jnp.transpose(ggrad[...])

    halo_copy.wait_recv()
    ext[tokens : tokens + 8, :] = jnp.where(sp < n_sp - 1, halo[...], 0.0)
    reach = taps_ref.shape[0] - 1
    tap_values = taps_ref[...].astype(f32)
    conv_grad = tap_values[0:1, :] * ext[reach : reach + tokens, :]
    for j in range(1, reach + 1):
        conv_grad = conv_grad + tap_values[j : j + 1, :] * ext[reach - j : reach - j + tokens, :]
    gci_ref[...] = (conv_grad * cg_ref[...].astype(f32)).astype(bf16)
    gcg_ref[...] = (conv_grad * ci_ref[...].astype(f32)).astype(bf16)

    def turn(j, carry):
        sl = pl.ds(pl.multiple_of(j * dcols, dcols), dcols)
        saved_t[sl, :] = jnp.transpose(saved[:, sl])
        return carry

    lax.fori_loop(0, width // dcols, turn, 0)
    wd_load.wait()

    def backward(i):
        sl = pair_rows(order[i])
        relay(eg, sl, egs_s, egs_r, 3 * i)
        arrive(eg, sl, egs_s, egs_r, 3 * i)
        act_grad = dot_nt(eg[sl, :], wd[...])
        g = (act_grad * fac_g[sl, :]).astype(bf16)
        u = (act_grad * fac_u[sl, :]).astype(bf16)
        ggrad[sl, :] = g
        ugrad[sl, :] = u

        def term(m):
            j = cols(m)
            terms[sl, j] = (dot_nt(g, wg[j, :]) + dot_nt(u, wu[j, :])).astype(bf16)

        for y in range(2):
            there = y * 2 + (1 - core)
            term(there)
            send(
                remote(
                    terms.at[sl, cols(there)],
                    px.at[sl, y * dcols : (y + 1) * dcols],
                    d2d_s.at[2 * i + y],
                    d2d_r.at[2 * i + y],
                    sp,
                    partner,
                )
            )
        for y in range(2):
            term(y * 2 + core)

    def pass_on(i):
        sl = pair_rows(order[i])
        for y in range(2):
            region = px.at[sl, y * dcols : (y + 1) * dcols]
            remote(
                region, region, d2d_s.at[2 * i + y], d2d_r.at[2 * i + y], sp, partner
            ).wait_recv()
        far = terms[sl, cols(across)].astype(f32) + px[sl, cols(1 - chip)].astype(f32)
        ysend[sl, :] = far.astype(bf16)
        send(remote(ysend.at[sl, :], yrecv.at[sl, :], y_s.at[i], y_r.at[i], sp, across))

    def give_back(i):
        sl = pair_rows(order[i])
        region = yrecv.at[sl, :]
        remote(region, region, y_s.at[i], y_r.at[i], sp, across).wait_recv()
        near = terms[sl, mine].astype(f32) + px[sl, cols(chip)].astype(f32)
        red[sl, :] = (near + yrecv[sl, :].astype(f32)).astype(bf16)
        for x in range(1 if i == 0 else 2):
            dest = plane * 2 + (1 - side) if i == 0 else order[i] * 2 + x
            send(
                remote(
                    red.at[block(dest), :],
                    ret.at[block(sp), :],
                    ret_s.at[dest],
                    ret_r.at[sp],
                    dest,
                    tp,
                )
            )
        if i == 0:
            ret[block(sp), :] = red[block(sp), :]

    backward(0)
    for i in range(1, planes):
        backward(i)
        pass_on(i - 1)
    pass_on(planes - 1)

    def down_tile(j, carry):
        sl = pl.ds(pl.multiple_of(j * dcols, dcols), dcols)
        gd_v[:, sl] = dot_nn(hidden_t[...], eg[:, sl]).astype(bf16)
        return carry

    give_back(0)
    lax.fori_loop(0, width // dcols, down_tile, 0)

    tile = width // 8

    def weight_tile(j, carry):
        sl = pl.ds(pl.multiple_of(j * tile, tile), tile)
        x = saved_t[sl, :]
        gg_v[sl, :] = dot_nn(x, ggrad[...]).astype(bf16)
        gu_v[sl, :] = dot_nn(x, ugrad[...]).astype(bf16)
        return carry

    done = 0
    for i in range(1, planes):
        give_back(i)
        if i < planes - 1:
            until = 8 * i // (planes - 1)
            lax.fori_loop(done, until, weight_tile, 0)
            done = until
    lax.fori_loop(done, 8, weight_tile, 0)

    total = proj[sp]
    for i in range(1, n_sp):
        source = lax.rem(sp + i, n_sp)
        region = precv.at[source]
        remote(region, region, proj_s.at[source], proj_r.at[source], source, tp).wait_recv()
        total = total + precv[source]
    gop_ref[...] = total

    for i in range(1, n_sp):
        source = lax.rem(sp + i, n_sp)
        region = ret.at[block(source), :]
        remote(region, region, ret_s.at[source], ret_r.at[source], source, tp).wait_recv()
    gr_ref[...] = dot_tn(sel[...], ret[...]).astype(bf16)
    for copy in pending:
        copy.wait_send()


def write_out(*refs):
    count = len(refs) // 2
    copies = [
        pltpu.make_async_copy(refs[n], refs[count + n], refs[-1].at[n]) for n in range(count)
    ]
    for copy in copies:
        copy.start()
    for copy in copies:
        copy.wait()


def fused(n_sp, layer_grad, routes, route_weights, expert_in, w_gate, w_up, w_down,
          conv_in, c_gate, b_gate, conv_out, taps, w_out):
    tokens, dcols = layer_grad.shape
    rows = expert_in.shape[1]
    width, units = w_gate.shape[1:]
    chans = conv_in.shape[1]
    share = width // n_sp
    planes = n_sp // 2
    any_spec = pl.BlockSpec(memory_space=pl.ANY)
    vmem = pl.BlockSpec(memory_space=pltpu.VMEM)
    dma = pltpu.SemaphoreType.DMA
    shape = jax.ShapeDtypeStruct
    kinds = (
        ((width, units), bf16),
        ((width, units), bf16),
        ((units, width), bf16),
        ((tokens, dcols), bf16),
        ((chans, share), f32),
        ((tokens, chans), bf16),
        ((tokens, chans), bf16),
        ((tokens, chans), bf16),
    )
    results = pl.pallas_call(
        functools.partial(fused_kernel, n_sp),
        out_shape=tuple(pltpu.VMEM(dims, dtype) for dims, dtype in kinds),
        in_specs=[any_spec, vmem, vmem] + [any_spec] * 4 + [vmem] * 5 + [any_spec],
        out_specs=(vmem,) * len(kinds),
        scratch_shapes=[
            pltpu.VMEM((width, units), bf16),
            pltpu.VMEM((width, units), bf16),
            pltpu.VMEM((units, width), bf16),
            pltpu.VMEM((chans, width), bf16),
            pltpu.VMEM((tokens, width), bf16),
            pltpu.VMEM((rows, width), bf16),
            pltpu.VMEM((width, rows), bf16),
            pltpu.VMEM((rows, width), bf16),
            pltpu.VMEM((rows, dcols), bf16),
            pltpu.VMEM((rows, tokens), bf16),
            pltpu.VMEM((n_sp, chans, share), f32),
            pltpu.VMEM((n_sp, chans, share), f32),
            pltpu.VMEM((tokens + 8, chans), f32),
            pltpu.VMEM((8, chans), f32),
            pltpu.VMEM((units, rows), bf16),
            pltpu.VMEM((rows, units), f32),
            pltpu.VMEM((rows, units), f32),
            pltpu.VMEM((rows, units), bf16),
            pltpu.VMEM((rows, units), bf16),
            pltpu.VMEM((rows, width), bf16),
            pltpu.VMEM((rows, 2 * dcols), bf16),
            pltpu.VMEM((rows, dcols), bf16),
            pltpu.VMEM((rows, dcols), bf16),
            pltpu.VMEM((rows, dcols), bf16),
            pltpu.VMEM((rows, dcols), bf16),
            dma((6,)),
            dma((3,)),
            dma((3,)),
            dma((3,)),
            dma((3,)),
            dma((n_sp,)),
            dma((n_sp,)),
            dma((3 * planes,)),
            dma((3 * planes,)),
            dma((n_sp,)),
            dma((n_sp,)),
            dma,
            dma,
            dma((2 * planes,)),
            dma((2 * planes,)),
            dma((planes,)),
            dma((planes,)),
            dma((n_sp,)),
            dma((n_sp,)),
        ],
        compiler_params=pltpu.CompilerParams(
            collective_id=0, has_side_effects=True, vmem_limit_bytes=52 * 1024 * 1024
        ),
    )(
        layer_grad,
        routes.T,
        route_weights.T,
        expert_in[0],
        w_gate[0],
        w_up[0],
        w_down[0],
        conv_in,
        c_gate,
        b_gate,
        conv_out,
        taps,
        w_out,
    )
    results = pl.pallas_call(
        write_out,
        out_shape=tuple(shape(dims, dtype) for dims, dtype in kinds),
        in_specs=[vmem] * len(kinds),
        out_specs=(any_spec,) * len(kinds),
        scratch_shapes=[dma((len(kinds),))],
        compiler_params=pltpu.CompilerParams(vmem_limit_bytes=2 * 1024 * 1024),
    )(*results)
    gate, up, down = results[:3]
    return (gate[None], up[None], down[None]) + tuple(results[3:])


def dispatching(n_sp, n_tp, layer_grad, routes, route_weights, expert_in, *others):
    tokens, dcols = layer_grad.shape
    cap = expert_in.shape[1] // n_sp
    chans = others[3].shape[1]
    fits = (
        n_tp == 4
        and n_sp % 2 == 0
        and n_sp >= 4
        and cap % 16 == 0
        and tokens % 128 == 0
        and dcols % 128 == 0
        and chans % 128 == 0
        and (dcols * n_tp) % (n_sp * 128) == 0
        and others[-2].shape[0] <= 9
    )
    if fits:
        return fused(n_sp, layer_grad, routes, route_weights, expert_in, *others)
    return per_device(layer_grad, routes, route_weights, expert_in, *others)


def solution(mesh):
    in_specs = (
        P("sp", "tp"),
        P("sp", None),
        P("sp", None),
        P("sp", None, "tp"),
        P("sp", None, "tp"),
        P("sp", None, "tp"),
        P("sp", "tp", None),
        P("sp", "tp"),
        P("sp", "tp"),
        P("sp", "tp"),
        P("sp", "tp"),
        P(None, "tp"),
        P("tp", None),
    )
    out_specs = (
        P("sp", None, "tp"),
        P("sp", None, "tp"),
        P("sp", "tp", None),
        P("sp", "tp"),
        P("tp", "sp"),
        P("sp", "tp"),
        P("sp", "tp"),
        P("sp", "tp"),
    )
    return jax.shard_map(
        functools.partial(dispatching, mesh.shape["sp"], mesh.shape["tp"]), mesh=mesh, in_specs=in_specs, out_specs=out_specs, check_vma=False
    )
```

profile of v0, /device:TPU:10, one launch (start us, length us, event | category | flops | bytes accessed | tf_op | source)
XLA Modules:
  0.0 81.5 jit_solution(8618130007530985452)
XLA Ops:
  0.6 78.0 %shard_map.188 = (bf16[2048,512]{1,0:T(8,128)(2,1)S(1)}, bf16[2048,512]{1,0:T(8,128)(2,1)S(1)}, bf16[512,2048]{1,0:T(8,128)(2,1)S(1)}, bf16[256,512]{1,0:T(8,128...) custom-call(bf16[256,512]{1,0:T(8,128)(2,1)} %lg_hbm.1, ...), custom_call_target="tpu_custom_call" | custom-call | tf_op jit(solution)/shard_map/pallas_call | solution.py:569
  78.6 2.9 %shard_map.189 = (bf16[2048,512]{1,0:T(8,128)(2,1)}, bf16[2048,512]{1,0:T(8,128)(2,1)}, bf16[512,2048]{1,0:T(8,128)(2,1)}, bf16[256,512]{1,0:T(8,128)(2,1)}, f32...) custom-call(bf16[2048,512]{1,0:T(8,128)(2,1)S(1)} %get-tuple-element.24.refs_0_, ...), custom_call_target="tpu_custom_call" | custom-call | tf_op jit(solution)/shard_map/pallas_call | solution.py:638
where the time goes:
time: 81.6 us; the launch traced here: 81.5 us
  Pallas kernels  80.8 us (99%)
    pallas_call x1, Pallas kernels, fused(): pl.pallas_call(functools.partial(fused_kernel, n_sp), out_shape=tuple((pl...  78 us
    pallas_call x1, Pallas kernels, fused(): pl.pallas_call(write_out, out_shape=tuple((shape(dims, dtype) for dims, d...  2.87 us

commit v1 on v0

v1 whole, which is shorter than its diff:
```python
import functools

import jax
import jax.numpy as jnp
from jax import lax
from jax.experimental import pallas as pl
from jax.experimental.pallas import tpu as pltpu
from jax.sharding import PartitionSpec as P

clamp_limit = 7.0
swish_alpha = 1.702


def passed_along(value, axis, steps):
    count = lax.axis_size(axis)
    leading, last = (max(0, -steps), min(count, count - steps))
    return lax.ppermute(value, axis, [(source, source + steps) for source in range(leading, last)])


def per_device(
    layer_grad,
    routes,
    route_weights,
    expert_in,
    w_gate,
    w_up,
    w_down,
    conv_in,
    c_gate,
    b_gate,
    conv_out,
    taps,
    w_out,
):
    sp_devices = lax.axis_size("sp")
    tok_rows = layer_grad.shape[0]
    top_count = routes.shape[1]
    capacity = expert_in.shape[1] // sp_devices
    full_grad = lax.all_gather(layer_grad, "tp", axis=1, tiled=True)
    flat_routes = routes.reshape(-1)
    onehot = (flat_routes[:, None] == jnp.arange(sp_devices, dtype=jnp.int32)[None, :]).astype(
        jnp.int32
    )
    slot_rank = jnp.sum((jnp.cumsum(onehot, axis=0) - 1) * onehot, axis=1)
    slot_index = flat_routes * capacity + slot_rank
    weights = route_weights[:, :, None]
    scaled = (weights * layer_grad[:, None, :].astype(jnp.float32)).astype(jnp.bfloat16)
    scaled = scaled.reshape(tok_rows * top_count, -1)
    buffer = (
        jnp.zeros((sp_devices * capacity, scaled.shape[1]), jnp.bfloat16).at[slot_index].set(scaled)
    )
    arrived = lax.all_to_all(
        buffer.reshape(sp_devices, capacity, -1), "sp", split_axis=0, concat_axis=0, tiled=True
    )
    expert_grad, saved_rows = (
        lax.all_gather(arrived.reshape(sp_devices * capacity, -1), "tp", axis=1, tiled=True),
        lax.all_gather(expert_in[0], "tp", axis=1, tiled=True),
    )
    gate_weight = w_gate[0]
    up_weight = w_up[0]
    down_weight = w_down[0]
    gate_pre = jnp.dot(saved_rows, gate_weight, preferred_element_type=jnp.float32)
    up_pre = jnp.dot(saved_rows, up_weight, preferred_element_type=jnp.float32)
    gate_cut = jnp.minimum(gate_pre, clamp_limit)
    up_cut = jnp.clip(up_pre, -clamp_limit, clamp_limit)
    sigmoid_gate = jax.nn.sigmoid(swish_alpha * gate_cut)
    hidden = ((up_cut + 1.0) * gate_cut * sigmoid_gate).astype(jnp.bfloat16)
    act_grad = jnp.einsum("rd,fd->rf", expert_grad, down_weight, preferred_element_type=jnp.float32)
    grad_down = jnp.einsum(
        "rf,rd->fd", hidden, expert_grad, preferred_element_type=jnp.float32
    ).astype(jnp.bfloat16)
    slope = sigmoid_gate + swish_alpha * gate_cut * sigmoid_gate * (1.0 - sigmoid_gate)
    gate_grad = jnp.where(gate_pre < clamp_limit, act_grad * (up_cut + 1.0) * slope, 0.0).astype(
        jnp.bfloat16
    )
    up_grad = jnp.where(
        jnp.abs(up_pre) < clamp_limit, act_grad * gate_cut * sigmoid_gate, 0.0
    ).astype(jnp.bfloat16)
    grad_gate = jnp.einsum(
        "rd,rf->df", saved_rows, gate_grad, preferred_element_type=jnp.float32
    ).astype(jnp.bfloat16)
    grad_up = jnp.einsum(
        "rd,rf->df", saved_rows, up_grad, preferred_element_type=jnp.float32
    ).astype(jnp.bfloat16)
    partial_value = jnp.einsum(
        "rf,df->rd", gate_grad, gate_weight, preferred_element_type=jnp.float32
    )
    partial_value = partial_value + jnp.einsum(
        "rf,df->rd", up_grad, up_weight, preferred_element_type=jnp.float32
    )
    rounded_terms = partial_value.astype(jnp.bfloat16)
    reduced = (
        lax.psum_scatter(rounded_terms, "tp", scatter_dimension=1, tiled=True)
        .astype(jnp.float32)
        .astype(jnp.bfloat16)
    )
    returned = lax.all_to_all(
        reduced.reshape(sp_devices, capacity, -1), "sp", split_axis=0, concat_axis=0, tiled=True
    )
    returned = returned.reshape(sp_devices * capacity, -1)
    picked = returned[slot_index]
    picked = picked.reshape(tok_rows, top_count, -1)
    grad_routed = jnp.sum(picked.astype(jnp.float32), axis=1).astype(jnp.bfloat16)
    mixer_grad = jnp.einsum("td,cd->tc", full_grad, w_out, preferred_element_type=jnp.float32)
    mixed = (b_gate.astype(jnp.float32) * conv_out.astype(jnp.float32)).astype(jnp.bfloat16)
    projected = lax.psum_scatter(
        jnp.einsum("td,tc->dc", full_grad, mixed, preferred_element_type=jnp.float32),
        "sp",
        scatter_dimension=0,
        tiled=True,
    )
    grad_out_proj = projected.T
    out_grad = mixer_grad * b_gate.astype(jnp.float32)
    tap_reach = taps.shape[0] - 1
    following = passed_along(out_grad[:tap_reach], "sp", -1)
    extended = jnp.concatenate([out_grad, following], axis=0)
    tap_values = taps.astype(jnp.float32)
    conv_grad = jnp.zeros_like(out_grad)
    for tap_index in range(tap_reach + 1):
        offset = tap_reach - tap_index
        conv_grad = conv_grad + tap_values[tap_index] * extended[offset : offset + tok_rows]
    grad_conv_in = (conv_grad * c_gate.astype(jnp.float32)).astype(jnp.bfloat16)
    grad_c_gate = (conv_grad * conv_in.astype(jnp.float32)).astype(jnp.bfloat16)
    grad_b_gate = (mixer_grad * conv_out.astype(jnp.float32)).astype(jnp.bfloat16)
    return (
        grad_gate[None],
        grad_up[None],
        grad_down[None],
        grad_routed,
        grad_out_proj,
        grad_conv_in,
        grad_c_gate,
        grad_b_gate,
    )


MESH = pl.DeviceIdType.MESH
bf16 = jnp.bfloat16
f32 = jnp.float32


def dot_nn(a, b):
    return jnp.dot(a, b, preferred_element_type=f32)


def dot_nt(a, b):
    return lax.dot_general(a, b, (((1,), (1,)), ((), ())), preferred_element_type=f32)


def dot_tn(a, b):
    return lax.dot_general(a, b, (((0,), (0,)), ((), ())), preferred_element_type=f32)


EXCHANGED = ("mirror",)
FIRST_SAVED = ("own", "mirror", "beyond")


def fused_kernel(
    n_sp,
    lg_hbm,
    rt_hbm,
    wt_hbm,
    ein_hbm,
    wg_hbm,
    wu_hbm,
    wd_hbm,
    ci_hbm,
    cg_hbm,
    bg_hbm,
    co_hbm,
    taps_hbm,
    wo_hbm,
    gg_v,
    gu_v,
    gd_v,
    sel,
    ret,
    gop_ref,
    gci_ref,
    gcg_ref,
    gbg_ref,
    wg,
    wu,
    wd,
    wg_t,
    wu_t,
    wd_t,
    wo,
    fg,
    saved,
    saved_t,
    eg,
    disp,
    disp_far,
    row_scale,
    proj,
    proj_x,
    proj_xr,
    proj_n,
    proj_nr,
    proj_a,
    proj_ar,
    ext,
    halo,
    hid,
    hidden_t,
    fac_g,
    fac_u,
    ggrad,
    ugrad,
    terms,
    px,
    ysend,
    yrecv,
    red,
    rt_ref,
    wt_ref,
    ci_ref,
    cg_ref,
    bg_ref,
    co_ref,
    taps_ref,
    load_s,
    lg_s,
    lg_r,
    ein_s,
    ein_r,
    disp_s,
    disp_r,
    far_s,
    far_r,
    egs_s,
    egs_r,
    swap_s,
    swap_r,
    proj_s,
    proj_r,
    halo_s,
    halo_r,
    d2d_s,
    d2d_r,
    y_s,
    y_r,
    ret_s,
    ret_r,
):
    sp = lax.axis_index("sp")
    tp = lax.axis_index("tp")
    core, chip = lax.rem(tp, 2), lax.div(tp, 2)
    partner = chip * 2 + (1 - core)
    across = (1 - chip) * 2 + core
    plane, side = lax.div(sp, 2), lax.rem(sp, 2)
    planes = n_sp // 2
    sibling = plane * 2 + (1 - side)
    near = plane + 1 - 2 * lax.rem(plane, 2)
    mirror = lax.rem(plane + 2, planes)
    beyond = lax.rem(near + 2, planes)
    rows, dcols = ein_hbm.shape
    cap = rows // n_sp
    pair = 2 * cap
    width = fg.shape[1]
    tokens = fg.shape[0]
    top = rt_hbm.shape[0]
    quads = {"own": plane, "near": near, "mirror": mirror, "beyond": beyond}
    index = {"own": 0, "near": 1, "mirror": 2, "beyond": 3}

    def cols(j):
        return pl.ds(pl.multiple_of(j * dcols, dcols), dcols)

    def block(b):
        return pl.ds(pl.multiple_of(b * cap, cap), cap)

    def pair_rows(q):
        return pl.ds(pl.multiple_of(q * pair, pair), pair)

    mine, other = cols(tp), cols(across)
    corner = cols((1 - chip) * 2 + (1 - core))

    def load(src, dst, n):
        copy = pltpu.make_async_copy(src, dst, load_s.at[n])
        copy.start()
        return copy

    def remote(src, dst, send, recv, to_sp, to_tp):
        return pltpu.make_async_remote_copy(
            src_ref=src,
            dst_ref=dst,
            send_sem=send,
            recv_sem=recv,
            device_id=(to_sp, to_tp),
            device_id_type=MESH,
        )

    barrier = pltpu.get_barrier_semaphore()
    pl.semaphore_signal(barrier, inc=1, device_id=(sp, partner), device_id_type=MESH)
    pl.semaphore_signal(barrier, inc=1, device_id=(sp, across), device_id_type=MESH)
    for i in range(1, n_sp):
        pl.semaphore_signal(
            barrier, inc=1, device_id=(lax.rem(sp + i, n_sp), tp), device_id_type=MESH
        )
    lg_load = load(lg_hbm, fg.at[:, mine], 0)
    ein_load = load(ein_hbm, saved.at[:, mine], 1)
    route_load = load(rt_hbm, rt_ref, 6)
    weight_load = load(wt_hbm, wt_ref, 7)
    mixer_loads = [
        load(bg_hbm, bg_ref, 8),
        load(co_hbm, co_ref, 9),
        load(ci_hbm, ci_ref, 10),
        load(cg_hbm, cg_ref, 11),
        load(taps_hbm, taps_ref, 12),
    ]
    wo_load = load(wo_hbm, wo, 2)
    wg_load = load(wg_hbm, wg, 3)
    wu_load = load(wu_hbm, wu, 4)
    wd_load = load(wd_hbm, wd, 5)
    pl.semaphore_wait(barrier, n_sp + 1)

    def send(copy):
        copy.start()
        return copy

    def sent(region, sem):
        remote(region, region, sem, sem, sp, partner).wait_send()

    def await_region(region, s_sem, r_sem):
        remote(region, region, s_sem, r_sem, sp, partner).wait_recv()

    def saved_across(name, sides=(0, 1)):
        i = index[name]
        for x in sides:
            sl = block(quads[name] * 2 + x)
            dst = saved.at[sl, mine]
            send(remote(ein_hbm.at[sl, :], dst, ein_s, ein_r.at[i], sp, across))

    def saved_relay(name):
        region, i = saved.at[pair_rows(quads[name]), other], index[name]
        await_region(region, ein_s, ein_r.at[i])
        send(remote(region, region, ein_s, ein_r.at[5 + i], sp, partner))

    def saved_arrive(name):
        region = saved.at[pair_rows(quads[name]), corner]
        await_region(region, ein_s, ein_r.at[5 + index[name]])

    def homes(name, sides=(0, 1)):
        return [sibling] if name == "own" else [quads[name] * 2 + x for x in sides]

    def rows_from(name):
        return block(sibling) if name == "own" else pair_rows(quads[name])

    send(remote(lg_hbm, fg.at[:, mine], lg_s, lg_r.at[0], sp, across))
    saved_across("mirror")
    saved_across("own")
    send(remote(lg_hbm, fg.at[:, mine], lg_s, lg_r.at[1], sp, partner))
    send(remote(ein_hbm, saved.at[:, mine], ein_s, ein_r.at[4], sp, partner))

    route_load.wait()
    weight_load.wait()
    expert_ids = lax.broadcasted_iota(jnp.int32, (n_sp, tokens), 0)
    named = jnp.zeros((n_sp, tokens), f32)
    weight = jnp.zeros((n_sp, tokens), f32)
    for k in range(top):
        hit = rt_ref[k : k + 1, :] == expert_ids
        named = jnp.where(hit, 1.0, named)
        weight = jnp.where(hit, wt_ref[k : k + 1, :], weight)
    earlier = (
        lax.broadcasted_iota(jnp.int32, (tokens, tokens), 0)
        < lax.broadcasted_iota(jnp.int32, (tokens, tokens), 1)
    )
    rank = dot_nn(named.astype(bf16), jnp.where(earlier, 1.0, 0.0).astype(bf16))
    rank = jnp.where(named > 0.0, rank, -1.0)
    slots = lax.broadcasted_iota(jnp.int32, (cap, tokens), 0).astype(f32)
    lg_load.wait()
    own_grad = fg[:, mine]
    for e in range(n_sp):
        chosen = slots == rank[e : e + 1, :]
        picks = jnp.where(chosen, 1.0, 0.0)
        row_weight = jnp.sum(jnp.where(chosen, weight[e : e + 1, :], 0.0), axis=1, keepdims=True)
        here = slice(e * cap, (e + 1) * cap)
        sel[here, :] = picks.astype(bf16)
        row_scale[here, :] = jnp.broadcast_to(row_weight, (cap, row_scale.shape[1]))
        disp[here, :] = (dot_nn(picks.astype(bf16), own_grad) * row_weight).astype(bf16)

    def dispatch(names):
        for name in names:
            for dest in homes(name):
                src, dst = disp.at[block(dest), :], eg.at[block(sp), mine]
                send(remote(src, dst, disp_s, disp_r.at[index[name]], dest, tp))

    def dispatch_far(names):
        for name in names:
            for dest in homes(name):
                src, dst = disp_far.at[block(dest), :], eg.at[block(sp), other]
                send(remote(src, dst, far_s, far_r.at[index[name]], dest, tp))

    def lg_relay():
        await_region(fg.at[:, other], lg_s, lg_r.at[0])
        send(remote(fg.at[:, other], fg.at[:, other], lg_s, lg_r.at[2], sp, partner))

    def select_across():
        far_grad = fg[:, other]
        for e in range(n_sp):
            here = slice(e * cap, (e + 1) * cap)
            disp_far[here, :] = (dot_nn(sel[here, :], far_grad) * row_scale[here, 0:1]).astype(bf16)

    def flip(src, dst):
        step = 512

        def part(j, carry):
            sl = pl.ds(pl.multiple_of(j * step, step), step)
            if src.shape[0] > src.shape[1]:
                dst[:, sl] = jnp.transpose(src[sl, :])
            else:
                dst[sl, :] = jnp.transpose(src[:, sl])
            return carry

        lax.fori_loop(0, width // step, part, 0)

    share = width // n_sp

    def mixer():
        wo_load.wait()
        for one in mixer_loads:
            one.wait()
        await_region(fg.at[:, cols(partner)], lg_s, lg_r.at[1])
        await_region(fg.at[:, corner], lg_s, lg_r.at[2])
        b_gate = bg_ref[...].astype(f32)
        conv_out = co_ref[...].astype(f32)
        mixer_grad = dot_nt(fg[...], wo[...])
        ext[0:tokens, :] = mixer_grad * b_gate
        gbg_ref[...] = (mixer_grad * conv_out).astype(bf16)
        before = lax.rem(sp + n_sp - 1, n_sp)
        halo_copy = send(remote(ext.at[0:8, :], halo, halo_s, halo_r, before, tp))
        mixed = (b_gate * conv_out).astype(bf16)
        for d in range(n_sp):
            proj[d % 2, d // 2] = dot_tn(mixed, fg[:, d * share : (d + 1) * share])
        proj_x[...] = proj[1 - side].astype(bf16)
        send(remote(proj_x, proj_xr, proj_s.at[0], proj_r.at[0], sibling, tp))
        return halo_copy

    def proj_near():
        await_region(proj_xr, proj_s.at[0], proj_r.at[0])
        for q in range(planes):
            proj[0, q] = proj[side, q] + proj_xr[q].astype(f32)
        proj_n[0] = proj[0, near].astype(bf16)
        proj_n[1] = proj[0, beyond].astype(bf16)
        send(remote(proj_n, proj_nr, proj_s.at[1], proj_r.at[1], near * 2 + side, tp))

    def proj_mirror():
        await_region(proj_nr, proj_s.at[1], proj_r.at[1])
        proj_a[...] = (proj[0, mirror] + proj_nr[1].astype(f32)).astype(bf16)
        send(remote(proj_a, proj_ar, proj_s.at[2], proj_r.at[2], mirror * 2 + side, tp))

    def proj_total():
        await_region(proj_ar, proj_s.at[2], proj_r.at[2])
        gop_ref[...] = proj[0, plane] + proj_nr[0].astype(f32) + proj_ar[...].astype(f32)

    def eg_mine(name):
        i, region = index[name], eg.at[pair_rows(quads[name]), mine]
        await_region(eg.at[rows_from(name), mine], disp_s, disp_r.at[i])
        if name in EXCHANGED:
            send(remote(region, region, swap_s, swap_r.at[EXCHANGED.index(name)], sp, across))
        send(remote(region, region, egs_s, egs_r.at[i], sp, partner))

    def eg_other(name):
        i, region = index[name], eg.at[pair_rows(quads[name]), other]
        if name in EXCHANGED:
            await_region(region, swap_s, swap_r.at[EXCHANGED.index(name)])
        else:
            await_region(eg.at[rows_from(name), other], far_s, far_r.at[i])
        send(remote(region, region, egs_s, egs_r.at[4 + i], sp, partner))

    def eg_arrive(name):
        sl, i = pair_rows(quads[name]), index[name]
        await_region(eg.at[sl, cols(partner)], egs_s, egs_r.at[i])
        await_region(eg.at[sl, corner], egs_s, egs_r.at[4 + i])

    def forward(name):
        sl = pair_rows(quads[name])
        x = saved[sl, :]
        gate_pre = dot_nn(x, wg[...])
        up_pre = dot_nn(x, wu[...])
        gate_cut = jnp.minimum(gate_pre, clamp_limit)
        up_cut = jnp.clip(up_pre, -clamp_limit, clamp_limit)
        sig = jax.nn.sigmoid(swish_alpha * gate_cut)
        base = gate_cut * sig
        slope = sig + swish_alpha * base * (1.0 - sig)
        hid[sl, :] = ((up_cut + 1.0) * base).astype(bf16)
        fac_g[sl, :] = jnp.where(gate_pre < clamp_limit, (up_cut + 1.0) * slope, 0.0)
        fac_u[sl, :] = jnp.where(jnp.abs(up_pre) < clamp_limit, base, 0.0)

    def backward(name):
        sl, i = pair_rows(quads[name]), index[name]
        act_grad = dot_nn(eg[sl, :], wd_t[...])
        g = (act_grad * fac_g[sl, :]).astype(bf16)
        u = (act_grad * fac_u[sl, :]).astype(bf16)
        ggrad[sl, :] = g
        ugrad[sl, :] = u

        def term(m):
            j = cols(m)
            terms[sl, j] = (dot_nn(g, wg_t[:, j]) + dot_nn(u, wu_t[:, j])).astype(bf16)

        for y in range(2):
            there = y * 2 + (1 - core)
            term(there)
            send(
                remote(
                    terms.at[sl, cols(there)],
                    px.at[sl, y * dcols : (y + 1) * dcols],
                    d2d_s,
                    d2d_r.at[i],
                    sp,
                    partner,
                )
            )
        for y in range(2):
            term(y * 2 + core)

    def pass_on(name):
        sl, i = pair_rows(quads[name]), index[name]
        await_region(px.at[sl, :], d2d_s, d2d_r.at[i])
        far = terms[sl, other].astype(f32) + px[sl, cols(1 - chip)].astype(f32)
        ysend[sl, :] = far.astype(bf16)
        send(remote(ysend.at[sl, :], yrecv.at[sl, :], y_s, y_r.at[i], sp, across))

    def add_up(name):
        sl, i = pair_rows(quads[name]), index[name]
        await_region(yrecv.at[sl, :], y_s, y_r.at[i])
        near_sum = terms[sl, mine].astype(f32) + px[sl, cols(chip)].astype(f32)
        red[sl, :] = (near_sum + yrecv[sl, :].astype(f32)).astype(bf16)
        if name == "own":
            ret[block(sp), :] = red[block(sp), :]

    def give(name, sides=(0, 1)):
        for dest in homes(name, sides):
            src, dst = red.at[block(dest), :], ret.at[block(sp), :]
            send(remote(src, dst, ret_s, ret_r.at[index[name]], dest, tp))

    def give_back(name):
        add_up(name)
        give(name)

    half = rows // 2

    def turn(h):
        part = pl.ds(pl.multiple_of(h * half, half), half)

        def step(j, carry):
            sl = pl.ds(pl.multiple_of(j * dcols, dcols), dcols)
            saved_t[sl, part] = jnp.transpose(saved[part, sl])
            return carry

        lax.fori_loop(0, width // dcols, step, 0)
        hidden_t[:, part] = jnp.transpose(hid[part, :])

    def down_tile(j, carry):
        sl = pl.ds(pl.multiple_of(j * dcols, dcols), dcols)
        gd_v[:, sl] = dot_nn(hidden_t[...], eg[:, sl]).astype(bf16)
        return carry

    tile = width // 8

    def weight_tile(j, carry):
        sl = pl.ds(pl.multiple_of(j * tile, tile), tile)
        x = saved_t[sl, :]
        gg_v[sl, :] = dot_nn(x, ggrad[...]).astype(bf16)
        gu_v[sl, :] = dot_nn(x, ugrad[...]).astype(bf16)
        return carry

    dispatch(("own", "mirror", "beyond", "near"))
    eg[block(sp), mine] = disp[block(sp), :]
    wd_load.wait()
    flip(wd, wd_t)
    wg_load.wait()
    flip(wg, wg_t)
    wu_load.wait()
    flip(wu, wu_t)
    lg_relay()
    select_across()
    dispatch_far(("own", "beyond", "near"))
    eg[block(sp), other] = disp_far[block(sp), :]
    eg_mine("mirror")
    saved_across("beyond")
    ein_load.wait()
    saved_relay("mirror")
    halo_copy = mixer()
    await_region(saved.at[:, cols(partner)], ein_s, ein_r.at[4])
    saved_arrive("mirror")
    forward("mirror")
    eg_mine("own")
    eg_other("own")
    saved_relay("own")
    saved_arrive("own")
    forward("own")
    eg_arrive("own")
    backward("own")
    eg_other("mirror")
    pass_on("own")
    eg_arrive("mirror")
    backward("mirror")
    pass_on("mirror")
    saved_across("near")
    saved_relay("beyond")
    eg_mine("beyond")
    saved_arrive("beyond")
    forward("beyond")
    turn(1 - lax.div(plane, 2))
    proj_near()
    eg_mine("near")
    eg_other("near")
    eg_other("beyond")
    give_back("mirror")
    eg_arrive("beyond")
    backward("beyond")
    pass_on("beyond")
    give_back("own")
    proj_mirror()
    saved_relay("near")
    saved_arrive("near")
    forward("near")
    eg_arrive("near")
    backward("near")
    pass_on("near")
    turn(lax.div(plane, 2))
    give_back("beyond")
    halo_copy.wait_recv()
    ext[tokens : tokens + 8, :] = jnp.where(sp < n_sp - 1, halo[...], 0.0)
    reach = taps_ref.shape[0] - 1
    tap_values = taps_ref[...].astype(f32)
    conv_grad = tap_values[0:1, :] * ext[reach : reach + tokens, :]
    for j in range(1, reach + 1):
        conv_grad = conv_grad + tap_values[j : j + 1, :] * ext[reach - j : reach - j + tokens, :]
    gci_ref[...] = (conv_grad * cg_ref[...].astype(f32)).astype(bf16)
    gcg_ref[...] = (conv_grad * ci_ref[...].astype(f32)).astype(bf16)
    lax.fori_loop(0, width // dcols, down_tile, 0)
    lax.fori_loop(0, 4, weight_tile, 0)
    give_back("near")
    lax.fori_loop(4, 8, weight_tile, 0)
    proj_total()
    def await_back(name):
        await_region(ret.at[rows_from(name), :], ret_s, ret_r.at[index[name]])
    await_back("mirror")
    await_back("beyond")
    await_back("near")
    await_back("own")
    sent(fg.at[:, 0 : 3 * dcols], lg_s)
    sent(saved.at[:, 0 : 3 * dcols], ein_s)
    sent(disp.at[0 : (n_sp - 1) * cap, :], disp_s)
    sent(disp_far.at[0 : (n_sp - 1 - 2 * len(EXCHANGED)) * cap, :], far_s)
    sent(eg.at[:, 0 : 2 * dcols], egs_s)
    for _ in EXCHANGED:
        sent(eg.at[0:pair, 0:dcols], swap_s)
    sent(px, d2d_s)
    sent(ysend, y_s)
    sent(red.at[0 : (n_sp - 1) * cap, :], ret_s)
    sent(proj_x, proj_s.at[0])
    sent(proj_n, proj_s.at[1])
    sent(proj_a, proj_s.at[2])
    halo_copy.wait_send()


def write_out(*refs):
    gate, up, down, sel, ret = refs[:5]
    ready, outs, total, sems = (gate, up, down) + refs[5:9], refs[9:17], refs[17], refs[18]
    copies = []
    for n, (src, dst) in enumerate(zip(ready, outs[:3] + outs[4:])):
        copies.append(pltpu.make_async_copy(src, dst, sems.at[n]))
    for copy in copies:
        copy.start()
    total[...] = dot_tn(sel[...], ret[...]).astype(bf16)
    last = pltpu.make_async_copy(total, outs[3], sems.at[len(copies)])
    last.start()
    for copy in copies + [last]:
        copy.wait()


def fused(n_sp, layer_grad, routes, route_weights, expert_in, w_gate, w_up, w_down,
          conv_in, c_gate, b_gate, conv_out, taps, w_out):
    tokens, dcols = layer_grad.shape
    rows = expert_in.shape[1]
    width, units = w_gate.shape[1:]
    chans = conv_in.shape[1]
    share = width // n_sp
    planes = n_sp // 2
    any_spec = pl.BlockSpec(memory_space=pl.ANY)
    vmem = pl.BlockSpec(memory_space=pltpu.VMEM)
    dma = pltpu.SemaphoreType.DMA
    shape = jax.ShapeDtypeStruct
    kinds = (
        ((width, units), bf16),
        ((width, units), bf16),
        ((units, width), bf16),
        ((rows, tokens), bf16),
        ((rows, dcols), bf16),
        ((chans, share), f32),
        ((tokens, chans), bf16),
        ((tokens, chans), bf16),
        ((tokens, chans), bf16),
    )
    results = pl.pallas_call(
        functools.partial(fused_kernel, n_sp),
        out_shape=tuple(pltpu.VMEM(dims, dtype) for dims, dtype in kinds),
        in_specs=[any_spec] * 13,
        out_specs=(vmem,) * len(kinds),
        scratch_shapes=[
            pltpu.VMEM((width, units), bf16),
            pltpu.VMEM((width, units), bf16),
            pltpu.VMEM((units, width), bf16),
            pltpu.VMEM((units, width), bf16),
            pltpu.VMEM((units, width), bf16),
            pltpu.VMEM((width, units), bf16),
            pltpu.VMEM((chans, width), bf16),
            pltpu.VMEM((tokens, width), bf16),
            pltpu.VMEM((rows, width), bf16),
            pltpu.VMEM((width, rows), bf16),
            pltpu.VMEM((rows, width), bf16),
            pltpu.VMEM((rows, dcols), bf16),
            pltpu.VMEM((rows, dcols), bf16),
            pltpu.VMEM((rows, 128), f32),
            pltpu.VMEM((2, planes, chans, share), f32),
            pltpu.VMEM((planes, chans, share), bf16),
            pltpu.VMEM((planes, chans, share), bf16),
            pltpu.VMEM((2, chans, share), bf16),
            pltpu.VMEM((2, chans, share), bf16),
            pltpu.VMEM((chans, share), bf16),
            pltpu.VMEM((chans, share), bf16),
            pltpu.VMEM((tokens + 8, chans), f32),
            pltpu.VMEM((8, chans), f32),
            pltpu.VMEM((rows, units), bf16),
            pltpu.VMEM((units, rows), bf16),
            pltpu.VMEM((rows, units), f32),
            pltpu.VMEM((rows, units), f32),
            pltpu.VMEM((rows, units), bf16),
            pltpu.VMEM((rows, units), bf16),
            pltpu.VMEM((rows, width), bf16),
            pltpu.VMEM((rows, 2 * dcols), bf16),
            pltpu.VMEM((rows, dcols), bf16),
            pltpu.VMEM((rows, dcols), bf16),
            pltpu.VMEM((rows, dcols), bf16),
            pltpu.VMEM(routes.shape[::-1], jnp.int32),
            pltpu.VMEM(routes.shape[::-1], f32),
            pltpu.VMEM((tokens, chans), bf16),
            pltpu.VMEM((tokens, chans), bf16),
            pltpu.VMEM((tokens, chans), bf16),
            pltpu.VMEM((tokens, chans), bf16),
            pltpu.VMEM(taps.shape, bf16),
            dma((13,)),
            dma,
            dma((3,)),
            dma,
            dma((9,)),
            dma,
            dma((4,)),
            dma,
            dma((4,)),
            dma,
            dma((8,)),
            dma,
            dma((2,)),
            dma((3,)),
            dma((3,)),
            dma,
            dma,
            dma,
            dma((4,)),
            dma,
            dma((4,)),
            dma,
            dma((4,)),
        ],
        compiler_params=pltpu.CompilerParams(
            collective_id=0, has_side_effects=True, vmem_limit_bytes=52 * 1024 * 1024
        ),
    )(
        layer_grad,
        routes.T,
        route_weights.T,
        expert_in[0],
        w_gate[0],
        w_up[0],
        w_down[0],
        conv_in,
        c_gate,
        b_gate,
        conv_out,
        taps,
        w_out,
    )
    results = pl.pallas_call(
        write_out,
        out_shape=tuple(
            shape(dims, dtype)
            for dims, dtype in kinds[:3] + (((tokens, dcols), bf16),) + kinds[5:]
        ),
        in_specs=[vmem] * len(kinds),
        out_specs=(any_spec,) * (len(kinds) - 1),
        scratch_shapes=[pltpu.VMEM((tokens, dcols), bf16), dma((len(kinds) - 1,))],
        compiler_params=pltpu.CompilerParams(vmem_limit_bytes=2 * 1024 * 1024),
    )(*results)
    gate, up, down = results[:3]
    return (gate[None], up[None], down[None]) + tuple(results[3:])


def dispatching(n_sp, n_tp, layer_grad, routes, route_weights, expert_in, *others):
    tokens, dcols = layer_grad.shape
    cap = expert_in.shape[1] // n_sp
    chans = others[3].shape[1]
    fits = (
        n_tp == 4
        and n_sp == 8
        and cap % 16 == 0
        and tokens % 128 == 0
        and dcols % 128 == 0
        and chans % 128 == 0
        and (dcols * n_tp) % (n_sp * 128) == 0
        and others[-2].shape[0] <= 9
    )
    if fits:
        return fused(n_sp, layer_grad, routes, route_weights, expert_in, *others)
    return per_device(layer_grad, routes, route_weights, expert_in, *others)


def solution(mesh):
    in_specs = (
        P("sp", "tp"),
        P("sp", None),
        P("sp", None),
        P("sp", None, "tp"),
        P("sp", None, "tp"),
        P("sp", None, "tp"),
        P("sp", "tp", None),
        P("sp", "tp"),
        P("sp", "tp"),
        P("sp", "tp"),
        P("sp", "tp"),
        P(None, "tp"),
        P("tp", None),
    )
    out_specs = (
        P("sp", None, "tp"),
        P("sp", None, "tp"),
        P("sp", "tp", None),
        P("sp", "tp"),
        P("tp", "sp"),
        P("sp", "tp"),
        P("sp", "tp"),
        P("sp", "tp"),
    )
    return jax.shard_map(
        functools.partial(dispatching, mesh.shape["sp"], mesh.shape["tp"]), mesh=mesh, in_specs=in_specs, out_specs=out_specs, check_vma=False
    )
```

time: 81.6 us -> 67 us (0.82)
  the two profiles are of different devices: /device:TPU:10 before, /device:TPU:0 now
where the time goes in v1:
time: 67 us; the launch traced here: 66.9 us
  Pallas kernels  66.2 us (99%)
    pallas_call x1, Pallas kernels, fused(): pl.pallas_call(functools.partial(fused_kernel, n_sp), out_shape=tuple((pl...  63.3 us
    pallas_call x1, Pallas kernels, fused(): pl.pallas_call(write_out, out_shape=tuple((shape(dims, dtype) for dims, d...  2.9 us

profile of v1, /device:TPU:0, one launch (start us, length us, event | category | flops | bytes accessed | tf_op | source)
XLA Modules:
  0.0 66.9 jit_solution(9289789253801323250)
XLA Ops:
  0.6 63.3 %shard_map.188 = (bf16[2048,512]{1,0:T(8,128)(2,1)S(1)}, bf16[2048,512]{1,0:T(8,128)(2,1)S(1)}, bf16[512,2048]{1,0:T(8,128)(2,1)S(1)}, bf16[768,256]{1,0:T(8,128...) custom-call(bf16[256,512]{1,0:T(8,128)(2,1)} %lg_hbm.1, ...), custom_call_target="tpu_custom_call" | custom-call | tf_op jit(solution)/shard_map/pallas_call | solution.py:700
  64.0 2.9 %shard_map.189 = (bf16[2048,512]{1,0:T(8,128)(2,1)}, bf16[2048,512]{1,0:T(8,128)(2,1)}, bf16[512,2048]{1,0:T(8,128)(2,1)}, bf16[256,512]{1,0:T(8,128)(2,1)}, f32...) custom-call(bf16[2048,512]{1,0:T(8,128)(2,1)S(1)} %get-tuple-element.25.refs_0_, ...), custom_call_target="tpu_custom_call" | custom-call | tf_op jit(solution)/shard_map/pallas_call | solution.py:789

commit v2 on v1

--- a/solution.py
+++ b/solution.py
@@ -152,6 +152,7 @@
 
 
 EXCHANGED = ("mirror",)
+EARLY = "own"
 FIRST_SAVED = ("own", "mirror", "beyond")
 
 
@@ -349,7 +350,7 @@
 
     send(remote(lg_hbm, fg.at[:, mine], lg_s, lg_r.at[0], sp, across))
     saved_across("mirror")
-    saved_across("own")
+    saved_across(EARLY)
     send(remote(lg_hbm, fg.at[:, mine], lg_s, lg_r.at[1], sp, partner))
     send(remote(ein_hbm, saved.at[:, mine], ein_s, ein_r.at[4], sp, partner))
 
@@ -516,9 +517,12 @@
         for y in range(2):
             term(y * 2 + core)
 
-    def pass_on(name):
+    def pass_on(name, sides=(0, 1)):
         sl, i = pair_rows(quads[name]), index[name]
-        await_region(px.at[sl, :], d2d_s, d2d_r.at[i])
+        if 0 in sides:
+            await_region(px.at[sl, :], d2d_s, d2d_r.at[i])
+        if len(sides) == 1:
+            sl = block(quads[name] * 2 + sides[0])
         far = terms[sl, other].astype(f32) + px[sl, cols(1 - chip)].astype(f32)
         ysend[sl, :] = far.astype(bf16)
         send(remote(ysend.at[sl, :], yrecv.at[sl, :], y_s, y_r.at[i], sp, across))
@@ -567,7 +571,7 @@
         gu_v[sl, :] = dot_nn(x, ugrad[...]).astype(bf16)
         return carry
 
-    dispatch(("own", "mirror", "beyond", "near"))
+    dispatch(("own", "mirror", "near", "beyond"))
     eg[block(sp), mine] = disp[block(sp), :]
     wd_load.wait()
     flip(wd, wd_t)
@@ -577,13 +581,14 @@
     flip(wu, wu_t)
     lg_relay()
     select_across()
-    dispatch_far(("own", "beyond", "near"))
+    dispatch_far(("own", "near", "beyond"))
     eg[block(sp), other] = disp_far[block(sp), :]
-    eg_mine("mirror")
-    saved_across("beyond")
     ein_load.wait()
     saved_relay("mirror")
     halo_copy = mixer()
+    eg_mine("mirror")
+    saved_across("near")
+    saved_across("beyond")
     await_region(saved.at[:, cols(partner)], ein_s, ein_r.at[4])
     saved_arrive("mirror")
     forward("mirror")
@@ -595,34 +600,31 @@
     eg_arrive("own")
     backward("own")
     eg_other("mirror")
-    pass_on("own")
+    eg_mine("near")
+    eg_other("near")
     eg_arrive("mirror")
     backward("mirror")
+    saved_relay("near")
     pass_on("mirror")
-    saved_across("near")
-    saved_relay("beyond")
-    eg_mine("beyond")
-    saved_arrive("beyond")
-    forward("beyond")
-    turn(1 - lax.div(plane, 2))
     proj_near()
-    eg_mine("near")
-    eg_other("near")
-    eg_other("beyond")
-    give_back("mirror")
-    eg_arrive("beyond")
-    backward("beyond")
-    pass_on("beyond")
-    give_back("own")
-    proj_mirror()
-    saved_relay("near")
     saved_arrive("near")
     forward("near")
     eg_arrive("near")
     backward("near")
     pass_on("near")
+    proj_mirror()
+    saved_relay("beyond")
+    eg_mine("beyond")
+    eg_other("beyond")
     turn(lax.div(plane, 2))
-    give_back("beyond")
+    saved_arrive("beyond")
+    forward("beyond")
+    give_back("mirror")
+    eg_arrive("beyond")
+    backward("beyond")
+    pass_on("beyond")
+    pass_on("own")
+    turn(1 - lax.div(plane, 2))
     halo_copy.wait_recv()
     ext[tokens : tokens + 8, :] = jnp.where(sp < n_sp - 1, halo[...], 0.0)
     reach = taps_ref.shape[0] - 1
@@ -633,16 +635,18 @@
     gci_ref[...] = (conv_grad * cg_ref[...].astype(f32)).astype(bf16)
     gcg_ref[...] = (conv_grad * ci_ref[...].astype(f32)).astype(bf16)
     lax.fori_loop(0, width // dcols, down_tile, 0)
+    give_back("near")
     lax.fori_loop(0, 4, weight_tile, 0)
-    give_back("near")
+    give_back("beyond")
     lax.fori_loop(4, 8, weight_tile, 0)
+    give_back("own")
     proj_total()
     def await_back(name):
         await_region(ret.at[rows_from(name), :], ret_s, ret_r.at[index[name]])
     await_back("mirror")
-    await_back("beyond")
     await_back("near")
     await_back("own")
+    await_back("beyond")
     sent(fg.at[:, 0 : 3 * dcols], lg_s)
     sent(saved.at[:, 0 : 3 * dcols], ein_s)
     sent(disp.at[0 : (n_sp - 1) * cap, :], disp_s)

time: 67 us -> 62.2 us (0.928)
  Pallas kernels: 66.2 us -> 61.4 us
    pallas_call x1, Pallas kernels: 63.3 us -> 58.5 us  [fused(): pl.pallas_call(functools.partial(fused_kernel, n_sp), out_shape=tuple((pl...]
where the time goes in v2:
time: 62.2 us; the launch traced here: 62 us
  Pallas kernels  61.4 us (99%)
  between operations  0.65 us (1%)
    pallas_call x1, Pallas kernels, fused(): pl.pallas_call(functools.partial(fused_kernel, n_sp), out_shape=tuple((pl...  58.5 us
    pallas_call x1, Pallas kernels, fused(): pl.pallas_call(write_out, out_shape=tuple((shape(dims, dtype) for dims, d...  2.9 us

profile of v2, /device:TPU:0, one launch (start us, length us, event | category | flops | bytes accessed | tf_op | source)
XLA Modules:
  0.0 62.0 jit_solution(1927253906764127528)
XLA Ops:
  0.6 58.5 %shard_map.188 = (bf16[2048,512]{1,0:T(8,128)(2,1)S(1)}, bf16[2048,512]{1,0:T(8,128)(2,1)S(1)}, bf16[512,2048]{1,0:T(8,128)(2,1)S(1)}, bf16[768,256]{1,0:T(8,128...) custom-call(bf16[256,512]{1,0:T(8,128)(2,1)} %lg_hbm.1, ...), custom_call_target="tpu_custom_call" | custom-call | tf_op jit(solution)/shard_map/pallas_call | solution.py:704
  59.1 2.9 %shard_map.189 = (bf16[2048,512]{1,0:T(8,128)(2,1)}, bf16[2048,512]{1,0:T(8,128)(2,1)}, bf16[512,2048]{1,0:T(8,128)(2,1)}, bf16[256,512]{1,0:T(8,128)(2,1)}, f32...) custom-call(bf16[2048,512]{1,0:T(8,128)(2,1)S(1)} %get-tuple-element.25.refs_0_, ...), custom_call_target="tpu_custom_call" | custom-call | tf_op jit(solution)/shard_map/pallas_call | solution.py:793

commit v3 on v2

--- a/solution.py
+++ b/solution.py
@@ -152,7 +152,10 @@
 
 
 EXCHANGED = ("mirror",)
-EARLY = "own"
+EARLY = "near"
+EARLY_SIDES = (0,)
+SWAP = 2
+BACK = 2
 FIRST_SAVED = ("own", "mirror", "beyond")
 
 
@@ -330,8 +333,8 @@
         i = index[name]
         for x in sides:
             sl = block(quads[name] * 2 + x)
-            dst = saved.at[sl, mine]
-            send(remote(ein_hbm.at[sl, :], dst, ein_s, ein_r.at[i], sp, across))
+            region = saved.at[sl, mine]
+            send(remote(region, region, ein_s, ein_r.at[i], sp, across))
 
     def saved_relay(name):
         region, i = saved.at[pair_rows(quads[name]), other], index[name]
@@ -342,17 +345,31 @@
         region = saved.at[pair_rows(quads[name]), corner]
         await_region(region, ein_s, ein_r.at[5 + index[name]])
 
-    def homes(name, sides=(0, 1)):
-        return [sibling] if name == "own" else [quads[name] * 2 + x for x in sides]
+    def homes(name, sides=(0, 1), order=SWAP):
+        if name == "own":
+            return [sibling]
+        if order == 2:
+            return [quads[name] * 2 + (1 - side) + x * (2 * side - 1) for x in sides]
+        if order == 1:
+            return [quads[name] * 2 + side + x * (1 - 2 * side) for x in sides]
+        if order == 3:
+            return [quads[name] * 2 + 1 - x for x in sides]
+        return [quads[name] * 2 + x for x in sides]
 
     def rows_from(name):
         return block(sibling) if name == "own" else pair_rows(quads[name])
 
-    send(remote(lg_hbm, fg.at[:, mine], lg_s, lg_r.at[0], sp, across))
-    saved_across("mirror")
-    saved_across(EARLY)
-    send(remote(lg_hbm, fg.at[:, mine], lg_s, lg_r.at[1], sp, partner))
-    send(remote(ein_hbm, saved.at[:, mine], ein_s, ein_r.at[4], sp, partner))
+    lg_load.wait()
+    lg_mine = fg.at[:, mine]
+    send(remote(lg_mine, lg_mine, lg_s, lg_r.at[0], sp, across))
+    send(remote(lg_mine, lg_mine, lg_s, lg_r.at[1], sp, partner))
+
+    def saved_start():
+        ein_load.wait()
+        saved_across("mirror")
+        saved_across(EARLY, EARLY_SIDES)
+        region = saved.at[:, mine]
+        send(remote(region, region, ein_s, ein_r.at[4], sp, partner))
 
     route_load.wait()
     weight_load.wait()
@@ -370,7 +387,6 @@
     rank = dot_nn(named.astype(bf16), jnp.where(earlier, 1.0, 0.0).astype(bf16))
     rank = jnp.where(named > 0.0, rank, -1.0)
     slots = lax.broadcasted_iota(jnp.int32, (cap, tokens), 0).astype(f32)
-    lg_load.wait()
     own_grad = fg[:, mine]
     for e in range(n_sp):
         chosen = slots == rank[e : e + 1, :]
@@ -536,7 +552,7 @@
             ret[block(sp), :] = red[block(sp), :]
 
     def give(name, sides=(0, 1)):
-        for dest in homes(name, sides):
+        for dest in homes(name, sides, BACK):
             src, dst = red.at[block(dest), :], ret.at[block(sp), :]
             send(remote(src, dst, ret_s, ret_r.at[index[name]], dest, tp))
 
@@ -572,6 +588,7 @@
         return carry
 
     dispatch(("own", "mirror", "near", "beyond"))
+    saved_start()
     eg[block(sp), mine] = disp[block(sp), :]
     wd_load.wait()
     flip(wd, wd_t)
@@ -581,50 +598,53 @@
     flip(wu, wu_t)
     lg_relay()
     select_across()
-    dispatch_far(("own", "near", "beyond"))
+    dispatch_far(("near", "own", "beyond"))
     eg[block(sp), other] = disp_far[block(sp), :]
-    ein_load.wait()
     saved_relay("mirror")
+    eg_mine("mirror")
+    saved_across("near", (1,))
+    saved_across("beyond")
     halo_copy = mixer()
-    eg_mine("mirror")
-    saved_across("near")
-    saved_across("beyond")
     await_region(saved.at[:, cols(partner)], ein_s, ein_r.at[4])
     saved_arrive("mirror")
     forward("mirror")
+    eg_other("mirror")
+    eg_arrive("mirror")
+    backward("mirror")
+    proj_near()
+    saved_relay("near")
+    eg_mine("near")
+    eg_other("near")
+    pass_on("mirror")
+    saved_across("own")
+    saved_arrive("near")
+    forward("near")
+    saved_relay("beyond")
     eg_mine("own")
     eg_other("own")
+    eg_mine("beyond")
+    eg_arrive("near")
+    backward("near")
+    pass_on("near", (0,))
+    proj_mirror()
+    saved_arrive("beyond")
+    forward("beyond")
+    eg_other("beyond")
+    give_back("mirror")
+    eg_arrive("beyond")
+    backward("beyond")
+    pass_on("beyond")
+    pass_on("near", (1,))
     saved_relay("own")
+    turn(1 - lax.div(plane, 2))
     saved_arrive("own")
     forward("own")
     eg_arrive("own")
     backward("own")
-    eg_other("mirror")
-    eg_mine("near")
-    eg_other("near")
-    eg_arrive("mirror")
-    backward("mirror")
-    saved_relay("near")
-    pass_on("mirror")
-    proj_near()
-    saved_arrive("near")
-    forward("near")
-    eg_arrive("near")
-    backward("near")
-    pass_on("near")
-    proj_mirror()
-    saved_relay("beyond")
-    eg_mine("beyond")
-    eg_other("beyond")
+    pass_on("own")
+    give_back("beyond")
     turn(lax.div(plane, 2))
-    saved_arrive("beyond")
-    forward("beyond")
-    give_back("mirror")
-    eg_arrive("beyond")
-    backward("beyond")
-    pass_on("beyond")
-    pass_on("own")
-    turn(1 - lax.div(plane, 2))
+    give_back("near")
     halo_copy.wait_recv()
     ext[tokens : tokens + 8, :] = jnp.where(sp < n_sp - 1, halo[...], 0.0)
     reach = taps_ref.shape[0] - 1
@@ -635,17 +655,15 @@
     gci_ref[...] = (conv_grad * cg_ref[...].astype(f32)).astype(bf16)
     gcg_ref[...] = (conv_grad * ci_ref[...].astype(f32)).astype(bf16)
     lax.fori_loop(0, width // dcols, down_tile, 0)
-    give_back("near")
-    lax.fori_loop(0, 4, weight_tile, 0)
-    give_back("beyond")
-    lax.fori_loop(4, 8, weight_tile, 0)
+    lax.fori_loop(0, 1, weight_tile, 0)
     give_back("own")
+    lax.fori_loop(1, 8, weight_tile, 0)
     proj_total()
     def await_back(name):
         await_region(ret.at[rows_from(name), :], ret_s, ret_r.at[index[name]])
     await_back("mirror")
+    await_back("own")
     await_back("near")
-    await_back("own")
     await_back("beyond")
     sent(fg.at[:, 0 : 3 * dcols], lg_s)
     sent(saved.at[:, 0 : 3 * dcols], ein_s)

time: 62.2 us -> 61.9 us (level)
  no operation moved by 1% of the time
where the time goes in v3:
time: 61.9 us; the launch traced here: 61.7 us
  Pallas kernels  61.1 us (99%)
  between operations  0.65 us (1%)
    pallas_call x1, Pallas kernels, fused(): pl.pallas_call(functools.partial(fused_kernel, n_sp), out_shape=tuple((pl...  58.2 us
    pallas_call x1, Pallas kernels, fused(): pl.pallas_call(write_out, out_shape=tuple((shape(dims, dtype) for dims, d...  2.9 us

profile of v3, /device:TPU:0, one launch (start us, length us, event | category | flops | bytes accessed | tf_op | source)
XLA Modules:
  0.0 61.7 jit_solution(10111375198853060532)
XLA Ops:
  0.6 58.2 %shard_map.188 = (bf16[2048,512]{1,0:T(8,128)(2,1)S(1)}, bf16[2048,512]{1,0:T(8,128)(2,1)S(1)}, bf16[512,2048]{1,0:T(8,128)(2,1)S(1)}, bf16[768,256]{1,0:T(8,128...) custom-call(bf16[256,512]{1,0:T(8,128)(2,1)} %lg_hbm.1, ...), custom_call_target="tpu_custom_call" | custom-call | tf_op jit(solution)/shard_map/pallas_call | solution.py:722
  58.8 2.9 %shard_map.189 = (bf16[2048,512]{1,0:T(8,128)(2,1)}, bf16[2048,512]{1,0:T(8,128)(2,1)}, bf16[512,2048]{1,0:T(8,128)(2,1)}, bf16[256,512]{1,0:T(8,128)(2,1)}, f32...) custom-call(bf16[2048,512]{1,0:T(8,128)(2,1)S(1)} %get-tuple-element.25.refs_0_, ...), custom_call_target="tpu_custom_call" | custom-call | tf_op jit(solution)/shard_map/pallas_call | solution.py:811
